TPU v7x, 32 devices: a whole 2x2x4 slice. The times are simulated.
32 devices in a mesh: ep: 8 (over z, x), tp: 4 (over y, core).
Axes of the slice: x: 2, y: 2, z: 4, core: 2. Of those that a mesh axis runs over, the one named last changes fastest.
Arguments:
- queries: bfloat16 [6144, 1024], P('ep', 'tp'), may hold values from -6.5 to 6.5
- keys: bfloat16 [6144, 1024], P('ep', 'tp'), may hold values from -6.5 to 6.5
- values: bfloat16 [6144, 1024], P('ep', 'tp'), may hold values from -6 to 6
- cum_gate: float32 [6144, 16], P('ep', 'tp'), may hold values from -770 to 0, as said below
- head_gain: float32 [1024], P('tp'), may hold values from 0.1 to 1.9
- moe_in: bfloat16 [1024, 2048], P('ep'), may hold values from -6 to 6
- ffn_gain: float32 [2048], replicated, may hold values from 0.1 to 1.9
- routes: int32 [1024, 4], P('ep'), may hold values from 0 to 31, all different within a row; in each aligned block of 128 rows (0 to 127, 128 to 255, ...) at most 24 rows name the same one
- route_weight: float32 [1024, 4], P('ep'), may hold values from 0.2 to 1.2
- expert_gate: bfloat16 [32, 1024, 2048], P('ep', 'tp'), may hold values from -0.125 to 0.125
- expert_up: bfloat16 [32, 1024, 2048], P('ep', 'tp'), may hold values from -0.125 to 0.125
- expert_down: bfloat16 [32, 1024, 2048], P('ep', 'tp'), may hold values from -0.25 to 0.25
- shared_gate: bfloat16 [512, 2048], P('tp'), may hold values from -0.125 to 0.125
- shared_up: bfloat16 [512, 2048], P('tp'), may hold values from -0.125 to 0.125
- shared_down: bfloat16 [512, 2048], P('tp'), may hold values from -0.375 to 0.375
Outputs:
- mixed: bfloat16 [6144, 1024], P('ep', 'tp')
- expert_out: bfloat16 [1024, 2048], P('ep', 'tp')
Inputs may be any that keep to these rules, and one draw needn't show every extreme that they name: `routes`: in each aligned block of 128 rows (the tokens of one index of ep) no expert is named by more than 24 rows, a bound that some block reaches; a row names 4 different experts. Each head's cum_gate never rises from one position to the next.
All inputs are finite; a program needn't handle non-finite values.
Results may differ from a plain program's by a relative error of at most 0.019.
Values may be sent and summed in bfloat16 or wider, within the bound.
A program may use at most 128 MiB of HBM per device.

v0:
```python
import math
import jax
import jax.numpy as jnp
from jax import lax
from jax.sharding import PartitionSpec as P

NORM_EPSILON = 1e-06


def keep_same(state_pair):
    return state_pair


def attend(queries, keys, values, cum_gate, head_gain):
    row_count, head_width = queries.shape
    head_count = cum_gate.shape[1]
    head_size = head_width // head_count
    score_scale = head_size ** (-0.5)
    first_row = lax.axis_index("ep") * row_count
    last_row = first_row + row_count - 1
    query_heads = queries.reshape(row_count, head_count, head_size)
    query_pos = first_row + jnp.arange(row_count, dtype=jnp.int32)
    query_gate = cum_gate.T
    all_gates = lax.all_gather(cum_gate, "ep", axis=0, tiled=True)
    start_state = (
        jnp.full((head_count, row_count), -1e30, jnp.float32),
        jnp.zeros((row_count, head_count, head_size), jnp.float32),
    )
    key_piece = lax.all_gather(keys, "ep", axis=0, tiled=True)
    value_piece = lax.all_gather(values, "ep", axis=0, tiled=True)
    piece_len = key_piece.shape[0]
    block_len = math.gcd(piece_len, 512)

    def visit(block_num, state_pair):
        offset = block_num * block_len

        def update(pair_in):
            running, weighted = pair_in
            key_block = lax.dynamic_slice_in_dim(key_piece, offset, block_len, 0).reshape(
                block_len, head_count, head_size
            )
            value_block = lax.dynamic_slice_in_dim(value_piece, offset, block_len, 0).reshape(
                block_len, head_count, head_size
            )
            key_gate = lax.dynamic_slice_in_dim(all_gates, offset, block_len, 0).T
            key_pos = offset + jnp.arange(block_len, dtype=jnp.int32)
            scores = (
                jnp.einsum(
                    "qhd,khd->hqk", query_heads, key_block, preferred_element_type=jnp.float32
                )
                * score_scale
            )
            scores = scores + query_gate[:, :, None] - key_gate[:, None, :]
            scores = jnp.where(key_pos[None, None, :] <= query_pos[None, :, None], scores, -jnp.inf)
            new_peak = jnp.maximum(running, jnp.max(scores, axis=2))
            weights = jnp.exp(scores - new_peak[:, :, None]).astype(jnp.bfloat16)
            shrink = jnp.exp(running - new_peak).T
            weighted = weighted * shrink[:, :, None] + jnp.einsum(
                "hqk,khd->qhd", weights, value_block, preferred_element_type=jnp.float32
            )
            return (new_peak, weighted)

        return lax.cond(offset <= last_row, update, keep_same, state_pair)

    running, weighted = lax.fori_loop(0, piece_len // block_len, visit, start_state)
    mean_square = jnp.mean(weighted * weighted, axis=2, keepdims=True)
    normed = (
        weighted * lax.rsqrt(mean_square + NORM_EPSILON) * head_gain.reshape(head_count, head_size)
    )
    return normed.reshape(row_count, head_width).astype(jnp.bfloat16)


def slot_index(route_rows, experts, capacity):
    flat_routes = route_rows.reshape(-1)
    agreement_tally = (
        flat_routes[:, None] == jnp.arange(experts, dtype=jnp.int32)[None, :]
    ).astype(jnp.int32)
    earlier = jnp.sum((jnp.cumsum(agreement_tally, axis=0) - 1) * agreement_tally, axis=1)
    return flat_routes * capacity + earlier


def experts_half(
    moe_in,
    ffn_gain,
    routes,
    route_weight,
    expert_gate,
    expert_up,
    expert_down,
    shared_gate,
    shared_up,
    shared_down,
):
    tokens, model_width = moe_in.shape
    choose = routes.shape[1]
    per_group = expert_gate.shape[0]
    groups = lax.axis_size("ep")
    experts = per_group * groups
    capacity = max(2, 3 * tokens * choose // (2 * experts))
    slice_width = model_width // lax.axis_size("tp")
    source = moe_in.astype(jnp.float32)
    normed = (
        source
        * lax.rsqrt(jnp.mean(source * source, axis=1, keepdims=True) + NORM_EPSILON)
        * ffn_gain
    ).astype(jnp.bfloat16)
    shared_hidden = (
        jax.nn.silu(
            jnp.einsum("td,fd->tf", normed, shared_gate, preferred_element_type=jnp.float32)
        )
        * jnp.einsum("td,fd->tf", normed, shared_up, preferred_element_type=jnp.float32)
    ).astype(jnp.bfloat16)
    shared_term = jnp.dot(shared_hidden, shared_down, preferred_element_type=jnp.float32)
    slot_ids = slot_index(routes, experts, capacity)
    owner_row = (
        jnp.full((experts * capacity,), tokens, jnp.int32)
        .at[slot_ids]
        .set(jnp.arange(tokens * choose, dtype=jnp.int32) // choose)
    )
    padded = jnp.concatenate([normed, jnp.zeros((1, model_width), normed.dtype)], axis=0)
    own_columns = lax.dynamic_slice_in_dim(
        padded, lax.axis_index("tp") * slice_width, slice_width, 1
    )
    arrived = lax.all_to_all(own_columns[owner_row], "ep", split_axis=0, concat_axis=0, tiled=True)
    column_piece = lax.all_gather(arrived, "tp", axis=1, tiled=True)
    piece_len = column_piece.shape[1]
    arranged = column_piece.reshape(groups, per_group, capacity, piece_len)
    gate_value = jnp.einsum(
        "slcd,lfd->slcf", arranged, expert_gate, preferred_element_type=jnp.float32
    )
    up_value = jnp.einsum("slcd,lfd->slcf", arranged, expert_up, preferred_element_type=jnp.float32)
    hidden = (jax.nn.silu(gate_value) * up_value).astype(jnp.bfloat16)
    expert_term = jnp.einsum(
        "slcf,lfd->slcd", hidden, expert_down, preferred_element_type=jnp.float32
    ).reshape(groups * per_group * capacity, model_width)
    expert_sum, shared_sum = (
        lax.psum_scatter(
            expert_term.astype(jnp.bfloat16), "tp", scatter_dimension=1, tiled=True
        ).astype(jnp.float32),
        lax.psum_scatter(
            shared_term.astype(jnp.bfloat16), "tp", scatter_dimension=1, tiled=True
        ).astype(jnp.float32),
    )
    returned = lax.all_to_all(
        expert_sum.astype(jnp.bfloat16), "ep", split_axis=0, concat_axis=0, tiled=True
    )
    picked = returned[slot_ids].reshape(tokens, choose, slice_width).astype(jnp.float32)
    routed = jnp.sum(picked * route_weight[:, :, None], axis=1)
    return (shared_sum + routed).astype(jnp.bfloat16)


def on_device(
    queries,
    keys,
    values,
    cum_gate,
    head_gain,
    moe_in,
    ffn_gain,
    routes,
    route_weight,
    expert_gate,
    expert_up,
    expert_down,
    shared_gate,
    shared_up,
    shared_down,
):
    mixed = attend(queries, keys, values, cum_gate, head_gain)
    expert_out = experts_half(
        moe_in,
        ffn_gain,
        routes,
        route_weight,
        expert_gate,
        expert_up,
        expert_down,
        shared_gate,
        shared_up,
        shared_down,
    )
    return (mixed, expert_out)


def solution(mesh):
    in_specs = (
        P("ep", "tp"),
        P("ep", "tp"),
        P("ep", "tp"),
        P("ep", "tp"),
        P("tp"),
        P("ep", None),
        P(),
        P("ep", None),
        P("ep", None),
        P("ep", "tp", None),
        P("ep", "tp", None),
        P("ep", "tp", None),
        P("tp", None),
        P("tp", None),
        P("tp", None),
    )
    out_specs = (P("ep", "tp"), P("ep", "tp"))
    return jax.shard_map(
        on_device, mesh=mesh, in_specs=in_specs, out_specs=out_specs, check_vma=False
    )
```

profile of v0, /device:TPU:27, one launch (start us, length us, event | category | flops | bytes accessed | tf_op | source)
XLA Modules:
  0.0 309.0 jit_solution(3351411150945842040)
XLA Ops:
  9.8 1.2 fusion.44
  11.3 1.2 reduce-window.6
  12.8 2.4 scatter_custom_fusion
  15.3 1.2 fusion.46
  16.6 2.7 gather_fusion
  19.3 23.3 %all_to_all.24 = bf16[8,96,512]{2,1,0:T(8,128)(2,1)} all-to-all(bf16[8,96,512]{2,1,0:T(8,128)(2,1)S(1)} %bitcast.100), channel_id=1, replica_groups=mesh['ep'=8,'tp'=4] {'ep'}, dimensions={0} | all-to-all | bytes 1572864 | tf_op jit(solution)/shard_map/all_to_all | solution.py:124
  42.6 30.3 %all-gather.8.cloned.1.call-done = bf16[768,2048]{1,0:T(8,128)(2,1)} async-done(((bf16[768,512]{1,0:T(8,128)(2,1)}), bf16[768,2048]{1,0:T(8,128)(2,1)}) %all-gather.8.cloned.1.call-update) | async-done | bytes 3145744 | tf_op jit(solution)/shard_map/all_gather | solution.py:125
  73.0 4.7 %fusion.23 = f32[8,4,24,256]{3,2,0,1:T(8,128)S(1)} fusion(bf16[4,256,2048]{2,1,0:T(8,128)(2,1)} %param.28, bf16[8,4,24,2048]{3,2,1,0:T(8,128)(2,1)} %bitcast.109), kind=kOutput, calls=%fused_computation.33 | convolution fusion | flops 805306368 | bytes 8126464 | tf_op jit(solution)/shard_map/slcd,lfd->slcf/dot_general | solution.py:128
  77.6 8.5 %fusion.18 = bf16[8,4,24,2048]{3,2,0,1:T(8,128)(2,1)} fusion(bf16[4,256,2048]{2,1,0:T(8,128)(2,1)} %param.30, bf16[4,256,2048]{2,1,0:T(8,128)(2,1)} %param.29, bf16[8,4,24,2048]{3,2,1,0:T(8,128)(2,1)} %bitcast.110, f32[8,4,24,256]{3,2,0,1:T(8,128)S(1)} %fusion.23), kind=kOutput, calls=%fused_computation.27 | convolution fusion | flops 1613365248 | bytes 15466496 | tf_op jit(solution)/shard_map/slcf,lfd->slcd/dot_general | solution.py:133
  86.1 4.1 %copy.32 = bf16[8,4,24,2048]{3,2,1,0:T(8,128)(2,1)} copy(bf16[8,4,24,2048]{3,2,0,1:T(8,128)(2,1)} %fusion.18) | data formatting | bytes 6291456 | tf_op jit(solution)/shard_map/convert_element_type | solution.py:138
  92.3 35.2 %reduce-scatter.5.cloned.1.call-done = bf16[768,512]{1,0:T(8,128)(2,1)} async-done(((bf16[768,2048]{1,0:T(8,128)(2,1)}), bf16[768,512]{1,0:T(8,128)(2,1)}) %reduce-scatter.5.cloned.1.call-update) | async-done | bytes 786448 | tf_op jit(solution)/shard_map/reduce_scatter | solution.py:137
  127.5 5.4 %all-to-all-start.1 = ((bf16[8,96,512]{2,1,0:T(8,128)(2,1)}), bf16[8,96,512]{2,1,0:T(8,128)(2,1)S(1)}, u32[]{:S(2)}, u32[]{:S(2)}) async-start(bf16[8,96,512]{2,1,0:T(8,128)(2,1)} %bitcast.103), calls=%async_computation.3 | async-start | bytes 1572864 | tf_op jit(solution)/shard_map/all_to_all | solution.py:144
  133.3 1.6 convolution_convert_fusion
  135.3 44.6 %all_gather.13 = f32[6144,4]{0,1:T(4,128)S(1)} all-gather(f32[768,4]{0,1:T(4,128)S(1)} %copy-done.6), channel_id=1, replica_groups=mesh['ep'=8,'tp'=4] {'ep'}, dimensions={0}, use_global_device_ids=true | all-gather | bytes 110592 | tf_op jit(solution)/shard_map/all_gather | solution.py:24
  179.9 46.6 %all-gather.6.cloned.1.call-done = bf16[6144,256]{0,1:T(8,128)(2,1)} async-done(((bf16[768,256]{0,1:T(8,128)(2,1)}), bf16[6144,256]{0,1:T(8,128)(2,1)}) %all-gather.6.cloned.1.call-update) | async-done | bytes 3145744 | tf_op jit(solution)/shard_map/all_gather | solution.py:30
  226.6 69.5 %while.16 = (s32[]{:T(128)}, f32[4,768]{1,0:T(4,128)S(1)}, f32[768,4,64]{0,2,1:T(8,128)S(1)}, s32[]{:T(128)}, bf16[6144,256]{0,1:T(8,128)(2,1)}, /*index=5*/bf16...) while((s32[]{:T(128)}, f32[4,768]{1,0:T(4,128)S(1)}, ...), condition=%wide.region_4.5_spmd.clone, body=%wide.region_0.4_spmd.clone.sunk | while | flops 420745472 | bytes 17461568 | solution.py:65
  226.7 5.8 %conditional.3 = ((f32[4,768]{1,0:T(4,128)S(1)}, f32[768,4,64]{0,2,1:T(8,128)S(1)})) conditional(s32[]{:T(128)} %convert_element_type.106, (f32[4,768]{1,0:T(4,128)S(1)}, f32[768,4,64]{0,2,1:T(8,128)S(1)}) %tuple.50, (s32[]{:T(128)}, s32[]{:T(128)}, bf16[6144,256]{0,1:T(8,128)(2,1)}, bf16[768,4,64]{0,2,1:T(8,128)(2,1)S(1)}, f32[4,768]{1,0:T(4,128)S(1)}, ...), branch_computations={%region_1.0_spmd, %region_2.3_spmd} | conditional | flops 420745472 | bytes 17458250 | solution.py:63
  227.0 1.1 constant_dynamic-slice_fusion
  228.1 1.9 fusion.2
  230.0 2.4 fusion.6
  232.5 5.7 %conditional.3 = ((f32[4,768]{1,0:T(4,128)S(1)}, f32[768,4,64]{0,2,1:T(8,128)S(1)})) conditional(s32[]{:T(128)} %convert_element_type.106, (f32[4,768]{1,0:T(4,128)S(1)}, f32[768,4,64]{0,2,1:T(8,128)S(1)}) %tuple.50, (s32[]{:T(128)}, s32[]{:T(128)}, bf16[6144,256]{0,1:T(8,128)(2,1)}, bf16[768,4,64]{0,2,1:T(8,128)(2,1)S(1)}, f32[4,768]{1,0:T(4,128)S(1)}, ...), branch_computations={%region_1.0_spmd, %region_2.3_spmd} | conditional | flops 420745472 | bytes 17458250 | solution.py:63
  232.8 1.1 constant_dynamic-slice_fusion
  233.9 1.9 fusion.2
  235.8 2.4 fusion.6
  238.3 5.7 %conditional.3 = ((f32[4,768]{1,0:T(4,128)S(1)}, f32[768,4,64]{0,2,1:T(8,128)S(1)})) conditional(s32[]{:T(128)} %convert_element_type.106, (f32[4,768]{1,0:T(4,128)S(1)}, f32[768,4,64]{0,2,1:T(8,128)S(1)}) %tuple.50, (s32[]{:T(128)}, s32[]{:T(128)}, bf16[6144,256]{0,1:T(8,128)(2,1)}, bf16[768,4,64]{0,2,1:T(8,128)(2,1)S(1)}, f32[4,768]{1,0:T(4,128)S(1)}, ...), branch_computations={%region_1.0_spmd, %region_2.3_spmd} | conditional | flops 420745472 | bytes 17458250 | solution.py:63
  238.6 1.1 constant_dynamic-slice_fusion
  239.7 1.9 fusion.2
  241.6 2.4 fusion.6
  244.0 5.7 %conditional.3 = ((f32[4,768]{1,0:T(4,128)S(1)}, f32[768,4,64]{0,2,1:T(8,128)S(1)})) conditional(s32[]{:T(128)} %convert_element_type.106, (f32[4,768]{1,0:T(4,128)S(1)}, f32[768,4,64]{0,2,1:T(8,128)S(1)}) %tuple.50, (s32[]{:T(128)}, s32[]{:T(128)}, bf16[6144,256]{0,1:T(8,128)(2,1)}, bf16[768,4,64]{0,2,1:T(8,128)(2,1)S(1)}, f32[4,768]{1,0:T(4,128)S(1)}, ...), branch_computations={%region_1.0_spmd, %region_2.3_spmd} | conditional | flops 420745472 | bytes 17458250 | solution.py:63
  244.4 1.1 constant_dynamic-slice_fusion
  245.5 1.9 fusion.2
  247.4 2.4 fusion.6
  249.8 5.7 %conditional.3 = ((f32[4,768]{1,0:T(4,128)S(1)}, f32[768,4,64]{0,2,1:T(8,128)S(1)})) conditional(s32[]{:T(128)} %convert_element_type.106, (f32[4,768]{1,0:T(4,128)S(1)}, f32[768,4,64]{0,2,1:T(8,128)S(1)}) %tuple.50, (s32[]{:T(128)}, s32[]{:T(128)}, bf16[6144,256]{0,1:T(8,128)(2,1)}, bf16[768,4,64]{0,2,1:T(8,128)(2,1)S(1)}, f32[4,768]{1,0:T(4,128)S(1)}, ...), branch_computations={%region_1.0_spmd, %region_2.3_spmd} | conditional | flops 420745472 | bytes 17458250 | solution.py:63
  250.2 1.1 constant_dynamic-slice_fusion
  251.3 1.9 fusion.2
  253.2 2.4 fusion.6
  255.6 5.7 %conditional.3 = ((f32[4,768]{1,0:T(4,128)S(1)}, f32[768,4,64]{0,2,1:T(8,128)S(1)})) conditional(s32[]{:T(128)} %convert_element_type.106, (f32[4,768]{1,0:T(4,128)S(1)}, f32[768,4,64]{0,2,1:T(8,128)S(1)}) %tuple.50, (s32[]{:T(128)}, s32[]{:T(128)}, bf16[6144,256]{0,1:T(8,128)(2,1)}, bf16[768,4,64]{0,2,1:T(8,128)(2,1)S(1)}, f32[4,768]{1,0:T(4,128)S(1)}, ...), branch_computations={%region_1.0_spmd, %region_2.3_spmd} | conditional | flops 420745472 | bytes 17458250 | solution.py:63
  256.0 1.1 constant_dynamic-slice_fusion
  257.1 1.9 fusion.2
  259.0 2.4 fusion.6
  261.4 5.7 %conditional.3 = ((f32[4,768]{1,0:T(4,128)S(1)}, f32[768,4,64]{0,2,1:T(8,128)S(1)})) conditional(s32[]{:T(128)} %convert_element_type.106, (f32[4,768]{1,0:T(4,128)S(1)}, f32[768,4,64]{0,2,1:T(8,128)S(1)}) %tuple.50, (s32[]{:T(128)}, s32[]{:T(128)}, bf16[6144,256]{0,1:T(8,128)(2,1)}, bf16[768,4,64]{0,2,1:T(8,128)(2,1)S(1)}, f32[4,768]{1,0:T(4,128)S(1)}, ...), branch_computations={%region_1.0_spmd, %region_2.3_spmd} | conditional | flops 420745472 | bytes 17458250 | solution.py:63
  261.8 1.1 constant_dynamic-slice_fusion
  262.9 1.9 fusion.2
  264.8 2.4 fusion.6
  267.2 5.7 %conditional.3 = ((f32[4,768]{1,0:T(4,128)S(1)}, f32[768,4,64]{0,2,1:T(8,128)S(1)})) conditional(s32[]{:T(128)} %convert_element_type.106, (f32[4,768]{1,0:T(4,128)S(1)}, f32[768,4,64]{0,2,1:T(8,128)S(1)}) %tuple.50, (s32[]{:T(128)}, s32[]{:T(128)}, bf16[6144,256]{0,1:T(8,128)(2,1)}, bf16[768,4,64]{0,2,1:T(8,128)(2,1)S(1)}, f32[4,768]{1,0:T(4,128)S(1)}, ...), branch_computations={%region_1.0_spmd, %region_2.3_spmd} | conditional | flops 420745472 | bytes 17458250 | solution.py:63
  267.6 1.1 constant_dynamic-slice_fusion
  268.6 1.9 fusion.2
  270.6 2.4 fusion.6
  273.0 5.7 %conditional.3 = ((f32[4,768]{1,0:T(4,128)S(1)}, f32[768,4,64]{0,2,1:T(8,128)S(1)})) conditional(s32[]{:T(128)} %convert_element_type.106, (f32[4,768]{1,0:T(4,128)S(1)}, f32[768,4,64]{0,2,1:T(8,128)S(1)}) %tuple.50, (s32[]{:T(128)}, s32[]{:T(128)}, bf16[6144,256]{0,1:T(8,128)(2,1)}, bf16[768,4,64]{0,2,1:T(8,128)(2,1)S(1)}, f32[4,768]{1,0:T(4,128)S(1)}, ...), branch_computations={%region_1.0_spmd, %region_2.3_spmd} | conditional | flops 420745472 | bytes 17458250 | solution.py:63
  273.4 1.1 constant_dynamic-slice_fusion
  274.4 1.9 fusion.2
  276.4 2.4 fusion.6
  278.8 5.7 %conditional.3 = ((f32[4,768]{1,0:T(4,128)S(1)}, f32[768,4,64]{0,2,1:T(8,128)S(1)})) conditional(s32[]{:T(128)} %convert_element_type.106, (f32[4,768]{1,0:T(4,128)S(1)}, f32[768,4,64]{0,2,1:T(8,128)S(1)}) %tuple.50, (s32[]{:T(128)}, s32[]{:T(128)}, bf16[6144,256]{0,1:T(8,128)(2,1)}, bf16[768,4,64]{0,2,1:T(8,128)(2,1)S(1)}, f32[4,768]{1,0:T(4,128)S(1)}, ...), branch_computations={%region_1.0_spmd, %region_2.3_spmd} | conditional | flops 420745472 | bytes 17458250 | solution.py:63
  280.2 1.9 fusion.2
  282.1 2.4 fusion.6
  284.6 5.7 %conditional.3 = ((f32[4,768]{1,0:T(4,128)S(1)}, f32[768,4,64]{0,2,1:T(8,128)S(1)})) conditional(s32[]{:T(128)} %convert_element_type.106, (f32[4,768]{1,0:T(4,128)S(1)}, f32[768,4,64]{0,2,1:T(8,128)S(1)}) %tuple.50, (s32[]{:T(128)}, s32[]{:T(128)}, bf16[6144,256]{0,1:T(8,128)(2,1)}, bf16[768,4,64]{0,2,1:T(8,128)(2,1)S(1)}, f32[4,768]{1,0:T(4,128)S(1)}, ...), branch_computations={%region_1.0_spmd, %region_2.3_spmd} | conditional | flops 420745472 | bytes 17458250 | solution.py:63
  286.0 1.9 fusion.2
  287.9 2.4 fusion.6
  290.4 5.7 %conditional.3 = ((f32[4,768]{1,0:T(4,128)S(1)}, f32[768,4,64]{0,2,1:T(8,128)S(1)})) conditional(s32[]{:T(128)} %convert_element_type.106, (f32[4,768]{1,0:T(4,128)S(1)}, f32[768,4,64]{0,2,1:T(8,128)S(1)}) %tuple.50, (s32[]{:T(128)}, s32[]{:T(128)}, bf16[6144,256]{0,1:T(8,128)(2,1)}, bf16[768,4,64]{0,2,1:T(8,128)(2,1)S(1)}, f32[4,768]{1,0:T(4,128)S(1)}, ...), branch_computations={%region_1.0_spmd, %region_2.3_spmd} | conditional | flops 420745472 | bytes 17458250 | solution.py:63
  290.7 1.1 constant_dynamic-slice_fusion
  291.8 1.9 fusion.2
  293.7 2.4 fusion.6
  297.3 2.0 gather_fusion.1
  300.3 1.6 add_convert_fusion
  (137 shorter events, 13.5 us)
Async XLA Ops:
  8.0 125.3 %copy-start = (bf16[128,2048]{1,0:T(8,128)(2,1)S(1)}, bf16[128,2048]{1,0:T(8,128)(2,1)}, u32[]{:S(2)}) copy-start(bf16[128,2048]{1,0:T(8,128)(2,1)} %param.33) | copy-start | bytes 1572868
  8.0 65.0 %all-gather.8.cloned.1.call-start = ((), (), s32[]{:S(2)}) async-start(), calls=%async_computation.7 | async-start | bytes 3932160 | tf_op jit(solution)/shard_map/all_gather | solution.py:125
  42.6 84.9 %reduce-scatter.5.cloned.1.call-start = ((), (), s32[]{:S(2)}) async-start(), calls=%async_computation.8 | async-start | bytes 3932160 | tf_op jit(solution)/shard_map/reduce_scatter | solution.py:137
  86.1 4.2 %copy-start.3 = (bf16[768,256]{1,0:T(8,128)(2,1)S(1)}, bf16[768,256]{1,0:T(8,128)(2,1)}, u32[]{:S(2)}) copy-start(bf16[768,256]{1,0:T(8,128)(2,1)} %param.20) | copy-start | bytes 1179652
  86.1 5.2 %copy-start.4 = (bf16[768,256]{1,0:T(8,128)(2,1)S(1)}, bf16[768,256]{1,0:T(8,128)(2,1)}, u32[]{:S(2)}) copy-start(bf16[768,256]{1,0:T(8,128)(2,1)} %param.21) | copy-start | bytes 1179652
  90.2 42.8 %copy-start.1 = (bf16[128,2048]{1,0:T(8,128)(2,1)S(1)}, bf16[128,2048]{1,0:T(8,128)(2,1)}, u32[]{:S(2)}) copy-start(bf16[128,2048]{1,0:T(8,128)(2,1)} %param.31) | copy-start | bytes 1572868
  90.2 43.1 %copy-start.2 = (bf16[128,2048]{1,0:T(8,128)(2,1)S(1)}, bf16[128,2048]{1,0:T(8,128)(2,1)}, u32[]{:S(2)}) copy-start(bf16[128,2048]{1,0:T(8,128)(2,1)} %param.32) | copy-start | bytes 1572868
  90.2 44.7 %copy-start.5 = (bf16[768,256]{1,0:T(8,128)(2,1)S(1)}, bf16[768,256]{1,0:T(8,128)(2,1)}, u32[]{:S(2)}) copy-start(bf16[768,256]{1,0:T(8,128)(2,1)} %param.19) | copy-start | bytes 1179652
  90.2 44.8 %copy-start.8 = (f32[256]{0:T(256)S(1)}, f32[256]{0:T(256)}, u32[]{:S(2)}) copy-start(f32[256]{0:T(256)} %param.23) | copy-start | bytes 3076
  90.3 44.9 %copy-start.7 = (f32[128,4]{0,1:T(4,128)S(1)}, f32[128,4]{0,1:T(4,128)}, u32[]{:S(2)}) copy-start(f32[128,4]{0,1:T(4,128)} %param.27) | copy-start | bytes 6148
  90.3 45.0 %copy-start.6 = (f32[768,4]{0,1:T(4,128)S(1)}, f32[768,4]{0,1:T(4,128)}, u32[]{:S(2)}) copy-start(f32[768,4]{0,1:T(4,128)} %param.22) | copy-start | bytes 36868
  90.3 89.6 %all-gather.4.cloned.1.call-start = ((), (), s32[]{:S(2)}) async-start(), calls=%async_computation.4 | async-start | bytes 3538944 | tf_op jit(solution)/shard_map/all_gather | solution.py:29
  91.3 135.3 %all-gather.6.cloned.1.call-start = ((), (), s32[]{:S(2)}) async-start(), calls=%async_computation.5 | async-start | bytes 3538944 | tf_op jit(solution)/shard_map/all_gather | solution.py:30
  127.5 169.8 %all-to-all-start.1 = ((bf16[8,96,512]{2,1,0:T(8,128)(2,1)}), bf16[8,96,512]{2,1,0:T(8,128)(2,1)S(1)}, u32[]{:S(2)}, u32[]{:S(2)}) async-start(bf16[8,96,512]{2,1,0:T(8,128)(2,1)} %bitcast.103), calls=%async_computation.3 | async-start | bytes 1572864 | tf_op jit(solution)/shard_map/all_to_all | solution.py:144
  132.9 167.4 %reduce-scatter.3.cloned.1.call-start = ((), (), s32[]{:S(2)}) async-start(), calls=%async_computation.6 | async-start | bytes 655360 | tf_op jit(solution)/shard_map/reduce_scatter | solution.py:140
Sparse Core Ops, SparseCore 0:
  42.7 30.1 all-gather.7
  90.3 37.1 reduce-scatter.4
  136.2 22.2 reduce-scatter.2
Sparse Core Ops, SparseCore 1:
  93.6 71.5 all-gather.3
  167.2 59.4 all-gather.5
where the time goes:
time: 310 us; the launch traced here: 309 us
  waiting for transfers between devices  112 us (36%)
  blocking collectives  67.9 us (22%)
  matrix products  66.4 us (21%)
  local copies, waits for them, and re-layouts  29.2 us (9%)
  between operations  15.5 us (5%)
  other arithmetic  10.8 us (3%)
  starting transfers between devices  5.61 us (2%)
    all_gather x1, waiting for transfers between devices, attend(): value_piece = lax.all_gather(values, 'ep', axis=0, tiled=True)  46.6 us
    all_gather x1, blocking collectives, attend(): all_gates = lax.all_gather(cum_gate, 'ep', axis=0, tiled=True)  44.6 us
    reduce_scatter x1, waiting for transfers between devices, experts_half(): lax.psum_scatter(expert_term.astype(jnp.bfloat16), 'tp', scatter_dimensio...  35.2 us
    all_gather x1, waiting for transfers between devices, experts_half(): column_piece = lax.all_gather(arrived, 'tp', axis=1, tiled=True)  30.3 us
    dot_general x12, matrix products, update(): jnp.einsum('hqk,khd->qhd', weights, value_block, preferred_element_type=j...  28.6 us
    all_to_all x1, blocking collectives, experts_half(): lax.all_to_all(own_columns[owner_row], 'ep', split_axis=0, concat_axis=0,...  23.3 us
    dot_general x12, matrix products, update(): jnp.einsum('qhd,khd->hqk', query_heads, key_block, preferred_element_type...  22.8 us
    dynamic_slice x12, local copies, waits for them, and re-layouts, update(): lax.dynamic_slice_in_dim(value_piece, offset, block_len, 0)  12.9 us
  transfers between devices with their start and end apart: 6, of which 3 were waited for; matrix products, arithmetic and copies ran while one was open for 25% of the time, Pallas kernels for 0%

commit v1 on v0

--- a/solution.py
+++ b/solution.py
@@ -122,7 +122,7 @@
         padded, lax.axis_index("tp") * slice_width, slice_width, 1
     )
     arrived = lax.all_to_all(own_columns[owner_row], "ep", split_axis=0, concat_axis=0, tiled=True)
-    column_piece = lax.all_gather(arrived, "tp", axis=1, tiled=True)
+    column_piece = jnp.concatenate(lax.all_gather(arrived, "tp"), axis=1)
     piece_len = column_piece.shape[1]
     arranged = column_piece.reshape(groups, per_group, capacity, piece_len)
     gate_value = jnp.einsum(

time: 310 us -> 322 us (1.039)
  local copies, waits for them, and re-layouts: 29.2 us -> 41.3 us
    another operation x1 -> x2, local copies, waits for them, and re-layouts: 0.01 us -> 6.09 us  [the longest x1 6.08 us: experts_half(): arranged = column_piece.reshape(groups, per_group, capacity, piece_len)]
    reshape x0 -> x1, local copies, waits for them, and re-layouts: none -> 6 us  [experts_half(): column_piece = jnp.concatenate(lax.all_gather(arrived, 'tp'), axis=1)]
  transfers between devices with their start and end apart: 6 -> 6, of which waited for: 3 -> 3; matrix products, arithmetic and copies ran while one was open for 25% -> 24% of each run, Pallas kernels for 0% -> 0%
where the time goes in v1:
time: 322 us; the launch traced here: 321 us
  waiting for transfers between devices  112 us (35%)
  blocking collectives  67.9 us (21%)
  matrix products  66.4 us (21%)
  local copies, waits for them, and re-layouts  41.3 us (13%)
  between operations  15.5 us (5%)
  other arithmetic  10.8 us (3%)
  starting transfers between devices  5.61 us (2%)
    all_gather x1, waiting for transfers between devices, attend(): value_piece = lax.all_gather(values, 'ep', axis=0, tiled=True)  46.6 us
    all_gather x1, blocking collectives, attend(): all_gates = lax.all_gather(cum_gate, 'ep', axis=0, tiled=True)  44.6 us
    reduce_scatter x1, waiting for transfers between devices, experts_half(): lax.psum_scatter(expert_term.astype(jnp.bfloat16), 'tp', scatter_dimensio...  35.2 us
    all_gather x1, waiting for transfers between devices, experts_half(): column_piece = jnp.concatenate(lax.all_gather(arrived, 'tp'), axis=1)  30.3 us
    dot_general x12, matrix products, update(): jnp.einsum('hqk,khd->qhd', weights, value_block, preferred_element_type=j...  28.6 us
    all_to_all x1, blocking collectives, experts_half(): lax.all_to_all(own_columns[owner_row], 'ep', split_axis=0, concat_axis=0,...  23.3 us
    dot_general x12, matrix products, update(): jnp.einsum('qhd,khd->hqk', query_heads, key_block, preferred_element_type...  22.8 us
    dynamic_slice x12, local copies, waits for them, and re-layouts, update(): lax.dynamic_slice_in_dim(value_piece, offset, block_len, 0)  12.9 us
  transfers between devices with their start and end apart: 6, of which 3 were waited for; matrix products, arithmetic and copies ran while one was open for 24% of the time, Pallas kernels for 0%

profile of v1, /device:TPU:27, one launch (start us, length us, event | category | flops | bytes accessed | tf_op | source)
XLA Modules:
  0.0 321.1 jit_solution(14433645308573526777)
XLA Ops:
  9.8 1.2 fusion.44
  11.3 1.2 reduce-window.6
  12.8 2.4 scatter_custom_fusion
  15.3 1.2 fusion.46
  16.6 2.7 gather_fusion
  19.3 23.3 %all_to_all.21 = bf16[8,96,512]{2,1,0:T(8,128)(2,1)} all-to-all(bf16[8,96,512]{2,1,0:T(8,128)(2,1)S(1)} %bitcast.100), channel_id=1, replica_groups=mesh['ep'=8,'tp'=4] {'ep'}, dimensions={0} | all-to-all | bytes 1572864 | tf_op jit(solution)/shard_map/all_to_all | solution.py:124
  42.6 30.3 %all-gather.8.cloned.1.call-done = bf16[4,768,512]{2,1,0:T(8,128)(2,1)} async-done(((bf16[1,768,512]{2,1,0:T(8,128)(2,1)}), bf16[4,768,512]{2,1,0:T(8,128)(2,1)}) %all-gather.8.cloned.1.call-update) | async-done | bytes 3145744 | tf_op jit(solution)/shard_map/all_gather | solution.py:125
  73.0 6.0 %copy.57 = bf16[768,4,512]{2,1,0:T(4,128)(2,1)} copy(bf16[768,4,512]{2,0,1:T(8,128)(2,1)} %bitcast.101) | data formatting | bytes 6291456 | tf_op jit(solution)/shard_map/reshape | solution.py:125
  79.0 6.1 %reshape_reshape.3 = bf16[8,4,24,2048]{3,2,1,0:T(8,128)(2,1)} reshape(bf16[768,4,512]{2,1,0:T(4,128)(2,1)} %copy.57) | data formatting | bytes 6291456 | tf_op jit(solution)/shard_map/reshape;reshape | solution.py:127
  85.1 4.7 %fusion.23 = f32[8,4,24,256]{3,2,0,1:T(8,128)S(1)} fusion(bf16[4,256,2048]{2,1,0:T(8,128)(2,1)} %param.28, bf16[8,4,24,2048]{3,2,1,0:T(8,128)(2,1)} %reshape_reshape.3), kind=kOutput, calls=%fused_computation.33 | convolution fusion | flops 805306368 | bytes 8126464 | tf_op jit(solution)/shard_map/slcd,lfd->slcf/dot_general | solution.py:128
  89.7 8.5 %fusion.18 = bf16[8,4,24,2048]{3,2,0,1:T(8,128)(2,1)} fusion(bf16[4,256,2048]{2,1,0:T(8,128)(2,1)} %param.30, bf16[4,256,2048]{2,1,0:T(8,128)(2,1)} %param.29, bf16[8,4,24,2048]{3,2,1,0:T(8,128)(2,1)} %reshape_reshape.3, f32[8,4,24,256]{3,2,0,1:T(8,128)S(1)} %fusion.23), kind=kOutput, calls=%fused_computation.27 | convolution fusion | flops 1613365248 | bytes 15466496 | tf_op jit(solution)/shard_map/slcf,lfd->slcd/dot_general | solution.py:133
  98.2 4.1 %copy.60 = bf16[8,4,24,2048]{3,2,1,0:T(8,128)(2,1)} copy(bf16[8,4,24,2048]{3,2,0,1:T(8,128)(2,1)} %fusion.18) | data formatting | bytes 6291456 | tf_op jit(solution)/shard_map/convert_element_type | solution.py:138
  104.4 35.2 %reduce-scatter.5.cloned.1.call-done = bf16[768,512]{1,0:T(8,128)(2,1)} async-done(((bf16[768,2048]{1,0:T(8,128)(2,1)}), bf16[768,512]{1,0:T(8,128)(2,1)}) %reduce-scatter.5.cloned.1.call-update) | async-done | bytes 786448 | tf_op jit(solution)/shard_map/reduce_scatter | solution.py:137
  139.6 5.4 %all-to-all-start.1 = ((bf16[8,96,512]{2,1,0:T(8,128)(2,1)}), bf16[8,96,512]{2,1,0:T(8,128)(2,1)S(1)}, u32[]{:S(2)}, u32[]{:S(2)}) async-start(bf16[8,96,512]{2,1,0:T(8,128)(2,1)} %bitcast.104), calls=%async_computation.3 | async-start | bytes 1572864 | tf_op jit(solution)/shard_map/all_to_all | solution.py:144
  145.4 1.6 convolution_convert_fusion
  147.4 44.6 %all_gather.16 = f32[6144,4]{0,1:T(4,128)S(1)} all-gather(f32[768,4]{0,1:T(4,128)S(1)} %copy-done.6), channel_id=1, replica_groups=mesh['ep'=8,'tp'=4] {'ep'}, dimensions={0}, use_global_device_ids=true | all-gather | bytes 110592 | tf_op jit(solution)/shard_map/all_gather | solution.py:24
  192.0 46.6 %all-gather.6.cloned.1.call-done = bf16[6144,256]{0,1:T(8,128)(2,1)} async-done(((bf16[768,256]{0,1:T(8,128)(2,1)}), bf16[6144,256]{0,1:T(8,128)(2,1)}) %all-gather.6.cloned.1.call-update) | async-done | bytes 3145744 | tf_op jit(solution)/shard_map/all_gather | solution.py:30
  238.7 69.5 %while.16 = (s32[]{:T(128)}, f32[4,768]{1,0:T(4,128)S(1)}, f32[768,4,64]{0,2,1:T(8,128)S(1)}, s32[]{:T(128)}, bf16[6144,256]{0,1:T(8,128)(2,1)}, /*index=5*/bf16...) while((s32[]{:T(128)}, f32[4,768]{1,0:T(4,128)S(1)}, ...), condition=%wide.region_4.5_spmd.clone, body=%wide.region_0.4_spmd.clone.sunk | while | flops 420745472 | bytes 17461568 | solution.py:65
  238.7 5.7 %conditional.3 = ((f32[4,768]{1,0:T(4,128)S(1)}, f32[768,4,64]{0,2,1:T(8,128)S(1)})) conditional(s32[]{:T(128)} %convert_element_type.106, (f32[4,768]{1,0:T(4,128)S(1)}, f32[768,4,64]{0,2,1:T(8,128)S(1)}) %tuple.52, (s32[]{:T(128)}, s32[]{:T(128)}, bf16[6144,256]{0,1:T(8,128)(2,1)}, bf16[768,4,64]{0,2,1:T(8,128)(2,1)S(1)}, f32[4,768]{1,0:T(4,128)S(1)}, ...), branch_computations={%region_1.0_spmd, %region_2.3_spmd} | conditional | flops 420745472 | bytes 17458250 | solution.py:63
  239.1 1.1 constant_dynamic-slice_fusion
  240.2 1.9 fusion.2
  242.1 2.4 fusion.6
  244.5 5.7 %conditional.3 = ((f32[4,768]{1,0:T(4,128)S(1)}, f32[768,4,64]{0,2,1:T(8,128)S(1)})) conditional(s32[]{:T(128)} %convert_element_type.106, (f32[4,768]{1,0:T(4,128)S(1)}, f32[768,4,64]{0,2,1:T(8,128)S(1)}) %tuple.52, (s32[]{:T(128)}, s32[]{:T(128)}, bf16[6144,256]{0,1:T(8,128)(2,1)}, bf16[768,4,64]{0,2,1:T(8,128)(2,1)S(1)}, f32[4,768]{1,0:T(4,128)S(1)}, ...), branch_computations={%region_1.0_spmd, %region_2.3_spmd} | conditional | flops 420745472 | bytes 17458250 | solution.py:63
  244.9 1.1 constant_dynamic-slice_fusion
  246.0 1.9 fusion.2
  247.9 2.4 fusion.6
  250.3 5.7 %conditional.3 = ((f32[4,768]{1,0:T(4,128)S(1)}, f32[768,4,64]{0,2,1:T(8,128)S(1)})) conditional(s32[]{:T(128)} %convert_element_type.106, (f32[4,768]{1,0:T(4,128)S(1)}, f32[768,4,64]{0,2,1:T(8,128)S(1)}) %tuple.52, (s32[]{:T(128)}, s32[]{:T(128)}, bf16[6144,256]{0,1:T(8,128)(2,1)}, bf16[768,4,64]{0,2,1:T(8,128)(2,1)S(1)}, f32[4,768]{1,0:T(4,128)S(1)}, ...), branch_computations={%region_1.0_spmd, %region_2.3_spmd} | conditional | flops 420745472 | bytes 17458250 | solution.py:63
  250.7 1.1 constant_dynamic-slice_fusion
  251.8 1.9 fusion.2
  253.7 2.4 fusion.6
  256.1 5.7 %conditional.3 = ((f32[4,768]{1,0:T(4,128)S(1)}, f32[768,4,64]{0,2,1:T(8,128)S(1)})) conditional(s32[]{:T(128)} %convert_element_type.106, (f32[4,768]{1,0:T(4,128)S(1)}, f32[768,4,64]{0,2,1:T(8,128)S(1)}) %tuple.52, (s32[]{:T(128)}, s32[]{:T(128)}, bf16[6144,256]{0,1:T(8,128)(2,1)}, bf16[768,4,64]{0,2,1:T(8,128)(2,1)S(1)}, f32[4,768]{1,0:T(4,128)S(1)}, ...), branch_computations={%region_1.0_spmd, %region_2.3_spmd} | conditional | flops 420745472 | bytes 17458250 | solution.py:63
  256.5 1.1 constant_dynamic-slice_fusion
  257.6 1.9 fusion.2
  259.5 2.4 fusion.6
  261.9 5.7 %conditional.3 = ((f32[4,768]{1,0:T(4,128)S(1)}, f32[768,4,64]{0,2,1:T(8,128)S(1)})) conditional(s32[]{:T(128)} %convert_element_type.106, (f32[4,768]{1,0:T(4,128)S(1)}, f32[768,4,64]{0,2,1:T(8,128)S(1)}) %tuple.52, (s32[]{:T(128)}, s32[]{:T(128)}, bf16[6144,256]{0,1:T(8,128)(2,1)}, bf16[768,4,64]{0,2,1:T(8,128)(2,1)S(1)}, f32[4,768]{1,0:T(4,128)S(1)}, ...), branch_computations={%region_1.0_spmd, %region_2.3_spmd} | conditional | flops 420745472 | bytes 17458250 | solution.py:63
  262.3 1.1 constant_dynamic-slice_fusion
  263.3 1.9 fusion.2
  265.3 2.4 fusion.6
  267.7 5.7 %conditional.3 = ((f32[4,768]{1,0:T(4,128)S(1)}, f32[768,4,64]{0,2,1:T(8,128)S(1)})) conditional(s32[]{:T(128)} %convert_element_type.106, (f32[4,768]{1,0:T(4,128)S(1)}, f32[768,4,64]{0,2,1:T(8,128)S(1)}) %tuple.52, (s32[]{:T(128)}, s32[]{:T(128)}, bf16[6144,256]{0,1:T(8,128)(2,1)}, bf16[768,4,64]{0,2,1:T(8,128)(2,1)S(1)}, f32[4,768]{1,0:T(4,128)S(1)}, ...), branch_computations={%region_1.0_spmd, %region_2.3_spmd} | conditional | flops 420745472 | bytes 17458250 | solution.py:63
  268.1 1.1 constant_dynamic-slice_fusion
  269.1 1.9 fusion.2
  271.1 2.4 fusion.6
  273.5 5.7 %conditional.3 = ((f32[4,768]{1,0:T(4,128)S(1)}, f32[768,4,64]{0,2,1:T(8,128)S(1)})) conditional(s32[]{:T(128)} %convert_element_type.106, (f32[4,768]{1,0:T(4,128)S(1)}, f32[768,4,64]{0,2,1:T(8,128)S(1)}) %tuple.52, (s32[]{:T(128)}, s32[]{:T(128)}, bf16[6144,256]{0,1:T(8,128)(2,1)}, bf16[768,4,64]{0,2,1:T(8,128)(2,1)S(1)}, f32[4,768]{1,0:T(4,128)S(1)}, ...), branch_computations={%region_1.0_spmd, %region_2.3_spmd} | conditional | flops 420745472 | bytes 17458250 | solution.py:63
  273.8 1.1 constant_dynamic-slice_fusion
  274.9 1.9 fusion.2
  276.8 2.4 fusion.6
  279.3 5.7 %conditional.3 = ((f32[4,768]{1,0:T(4,128)S(1)}, f32[768,4,64]{0,2,1:T(8,128)S(1)})) conditional(s32[]{:T(128)} %convert_element_type.106, (f32[4,768]{1,0:T(4,128)S(1)}, f32[768,4,64]{0,2,1:T(8,128)S(1)}) %tuple.52, (s32[]{:T(128)}, s32[]{:T(128)}, bf16[6144,256]{0,1:T(8,128)(2,1)}, bf16[768,4,64]{0,2,1:T(8,128)(2,1)S(1)}, f32[4,768]{1,0:T(4,128)S(1)}, ...), branch_computations={%region_1.0_spmd, %region_2.3_spmd} | conditional | flops 420745472 | bytes 17458250 | solution.py:63
  280.7 1.9 fusion.2
  282.6 2.4 fusion.6
  285.1 5.7 %conditional.3 = ((f32[4,768]{1,0:T(4,128)S(1)}, f32[768,4,64]{0,2,1:T(8,128)S(1)})) conditional(s32[]{:T(128)} %convert_element_type.106, (f32[4,768]{1,0:T(4,128)S(1)}, f32[768,4,64]{0,2,1:T(8,128)S(1)}) %tuple.52, (s32[]{:T(128)}, s32[]{:T(128)}, bf16[6144,256]{0,1:T(8,128)(2,1)}, bf16[768,4,64]{0,2,1:T(8,128)(2,1)S(1)}, f32[4,768]{1,0:T(4,128)S(1)}, ...), branch_computations={%region_1.0_spmd, %region_2.3_spmd} | conditional | flops 420745472 | bytes 17458250 | solution.py:63
  286.5 1.9 fusion.2
  288.4 2.4 fusion.6
  290.9 5.7 %conditional.3 = ((f32[4,768]{1,0:T(4,128)S(1)}, f32[768,4,64]{0,2,1:T(8,128)S(1)})) conditional(s32[]{:T(128)} %convert_element_type.106, (f32[4,768]{1,0:T(4,128)S(1)}, f32[768,4,64]{0,2,1:T(8,128)S(1)}) %tuple.52, (s32[]{:T(128)}, s32[]{:T(128)}, bf16[6144,256]{0,1:T(8,128)(2,1)}, bf16[768,4,64]{0,2,1:T(8,128)(2,1)S(1)}, f32[4,768]{1,0:T(4,128)S(1)}, ...), branch_computations={%region_1.0_spmd, %region_2.3_spmd} | conditional | flops 420745472 | bytes 17458250 | solution.py:63
  291.2 1.1 constant_dynamic-slice_fusion
  292.3 1.9 fusion.2
  294.2 2.4 fusion.6
  296.6 5.7 %conditional.3 = ((f32[4,768]{1,0:T(4,128)S(1)}, f32[768,4,64]{0,2,1:T(8,128)S(1)})) conditional(s32[]{:T(128)} %convert_element_type.106, (f32[4,768]{1,0:T(4,128)S(1)}, f32[768,4,64]{0,2,1:T(8,128)S(1)}) %tuple.52, (s32[]{:T(128)}, s32[]{:T(128)}, bf16[6144,256]{0,1:T(8,128)(2,1)}, bf16[768,4,64]{0,2,1:T(8,128)(2,1)S(1)}, f32[4,768]{1,0:T(4,128)S(1)}, ...), branch_computations={%region_1.0_spmd, %region_2.3_spmd} | conditional | flops 420745472 | bytes 17458250 | solution.py:63
  298.1 1.9 fusion.2
  300.0 2.4 fusion.6
  302.4 5.7 %conditional.3 = ((f32[4,768]{1,0:T(4,128)S(1)}, f32[768,4,64]{0,2,1:T(8,128)S(1)})) conditional(s32[]{:T(128)} %convert_element_type.106, (f32[4,768]{1,0:T(4,128)S(1)}, f32[768,4,64]{0,2,1:T(8,128)S(1)}) %tuple.52, (s32[]{:T(128)}, s32[]{:T(128)}, bf16[6144,256]{0,1:T(8,128)(2,1)}, bf16[768,4,64]{0,2,1:T(8,128)(2,1)S(1)}, f32[4,768]{1,0:T(4,128)S(1)}, ...), branch_computations={%region_1.0_spmd, %region_2.3_spmd} | conditional | flops 420745472 | bytes 17458250 | solution.py:63
  303.9 1.9 fusion.2
  305.8 2.4 fusion.6
  309.3 2.0 gather_fusion.1
  312.4 1.6 add_convert_fusion
  (139 shorter events, 15.6 us)
Async XLA Ops:
  8.0 137.4 %copy-start = (bf16[128,2048]{1,0:T(8,128)(2,1)S(1)}, bf16[128,2048]{1,0:T(8,128)(2,1)}, u32[]{:S(2)}) copy-start(bf16[128,2048]{1,0:T(8,128)(2,1)} %param.33) | copy-start | bytes 1572868
  8.0 65.0 %all-gather.8.cloned.1.call-start = ((), (), s32[]{:S(2)}) async-start(), calls=%async_computation.7 | async-start | bytes 3932160 | tf_op jit(solution)/shard_map/all_gather | solution.py:125
  42.6 97.0 %reduce-scatter.5.cloned.1.call-start = ((), (), s32[]{:S(2)}) async-start(), calls=%async_computation.8 | async-start | bytes 3932160 | tf_op jit(solution)/shard_map/reduce_scatter | solution.py:137
  98.2 4.2 %copy-start.3 = (bf16[768,256]{1,0:T(8,128)(2,1)S(1)}, bf16[768,256]{1,0:T(8,128)(2,1)}, u32[]{:S(2)}) copy-start(bf16[768,256]{1,0:T(8,128)(2,1)} %param.20) | copy-start | bytes 1179652
  98.2 5.2 %copy-start.4 = (bf16[768,256]{1,0:T(8,128)(2,1)S(1)}, bf16[768,256]{1,0:T(8,128)(2,1)}, u32[]{:S(2)}) copy-start(bf16[768,256]{1,0:T(8,128)(2,1)} %param.21) | copy-start | bytes 1179652
  102.3 42.8 %copy-start.1 = (bf16[128,2048]{1,0:T(8,128)(2,1)S(1)}, bf16[128,2048]{1,0:T(8,128)(2,1)}, u32[]{:S(2)}) copy-start(bf16[128,2048]{1,0:T(8,128)(2,1)} %param.31) | copy-start | bytes 1572868
  102.3 43.1 %copy-start.2 = (bf16[128,2048]{1,0:T(8,128)(2,1)S(1)}, bf16[128,2048]{1,0:T(8,128)(2,1)}, u32[]{:S(2)}) copy-start(bf16[128,2048]{1,0:T(8,128)(2,1)} %param.32) | copy-start | bytes 1572868
  102.3 44.7 %copy-start.5 = (bf16[768,256]{1,0:T(8,128)(2,1)S(1)}, bf16[768,256]{1,0:T(8,128)(2,1)}, u32[]{:S(2)}) copy-start(bf16[768,256]{1,0:T(8,128)(2,1)} %param.19) | copy-start | bytes 1179652
  102.3 44.9 %copy-start.8 = (f32[256]{0:T(256)S(1)}, f32[256]{0:T(256)}, u32[]{:S(2)}) copy-start(f32[256]{0:T(256)} %param.23) | copy-start | bytes 3076
  102.3 45.0 %copy-start.7 = (f32[128,4]{0,1:T(4,128)S(1)}, f32[128,4]{0,1:T(4,128)}, u32[]{:S(2)}) copy-start(f32[128,4]{0,1:T(4,128)} %param.27) | copy-start | bytes 6148
  102.3 45.1 %copy-start.6 = (f32[768,4]{0,1:T(4,128)S(1)}, f32[768,4]{0,1:T(4,128)}, u32[]{:S(2)}) copy-start(f32[768,4]{0,1:T(4,128)} %param.22) | copy-start | bytes 36868
  102.4 89.7 %all-gather.4.cloned.1.call-start = ((), (), s32[]{:S(2)}) async-start(), calls=%async_computation.4 | async-start | bytes 3538944 | tf_op jit(solution)/shard_map/all_gather | solution.py:29
  103.4 135.3 %all-gather.6.cloned.1.call-start = ((), (), s32[]{:S(2)}) async-start(), calls=%async_computation.5 | async-start | bytes 3538944 | tf_op jit(solution)/shard_map/all_gather | solution.py:30
  139.6 169.7 %all-to-all-start.1 = ((bf16[8,96,512]{2,1,0:T(8,128)(2,1)}), bf16[8,96,512]{2,1,0:T(8,128)(2,1)S(1)}, u32[]{:S(2)}, u32[]{:S(2)}) async-start(bf16[8,96,512]{2,1,0:T(8,128)(2,1)} %bitcast.104), calls=%async_computation.3 | async-start | bytes 1572864 | tf_op jit(solution)/shard_map/all_to_all | solution.py:144
  145.1 167.3 %reduce-scatter.3.cloned.1.call-start = ((), (), s32[]{:S(2)}) async-start(), calls=%async_computation.6 | async-start | bytes 655360 | tf_op jit(solution)/shard_map/reduce_scatter | solution.py:140
Sparse Core Ops, SparseCore 0:
  42.7 30.2 all-gather.7
  102.4 37.1 reduce-scatter.4
  148.3 22.1 reduce-scatter.2
Sparse Core Ops, SparseCore 1:
  105.6 71.4 all-gather.3
  179.2 59.4 all-gather.5
